TPU v7x, 32 devices: a whole 2x2x4 slice. The times are simulated.
32 devices in a mesh: sp: 8 (over z, y), dp: 4 (over x, core).
Axes of the slice: x: 2, y: 2, z: 4, core: 2. Of those that a mesh axis runs over, the one named last changes fastest.
Arguments:
- u_pre: bfloat16 [4, 8192, 2048], P('dp', 'sp'), may hold values from -6 to 6
- v_pre: bfloat16 [4, 8192, 2048], P('dp', 'sp'), may hold values from -6 to 6
- d_out: bfloat16 [4, 8192, 2048], P('dp', 'sp'), may hold values from -6 to 6
- w_mix: bfloat16 [16, 128, 128], replicated, may hold values from -0.5 to 0.5
- mix_bias: float32 [16, 128], replicated, may hold values from 0.1 to 1.9
- norm_gain: float32 [16, 128], replicated, may hold values from 0.1 to 1.9
- norm_shift: float32 [16, 128], replicated, may hold values from -3 to 3
- w_out: bfloat16 [2048, 2048], P('dp'), may hold values from -0.125 to 0.125
Outputs:
- grad_u: bfloat16 [4, 8192, 2048], P('dp', 'sp')
- grad_v: bfloat16 [4, 8192, 2048], P('dp', 'sp')
- grad_w_out: float32 [2048, 2048], P('dp')
- grad_w_mix: float32 [16, 128, 128], replicated
- grad_mix_bias: float32 [16, 128], replicated
- grad_gain: float32 [16, 128], replicated
- grad_shift: float32 [16, 128], replicated
All inputs are finite; a program needn't handle non-finite values.
Results may differ from a plain program's by a relative error of at most 0.012.
Values may be sent and summed in bfloat16 or wider, within the bound.
A program may use at most 192 MiB of HBM per device.

v0:
```python
import jax
import jax.numpy as jnp
from jax import lax
from jax.sharding import PartitionSpec as P

EPS = 1e-05


def mechanism(grad_s, u_pre, v_pre, w_mix, mix_bias, gain, shift):
    items, length, width = grad_s.shape
    groups, span = (w_mix.shape[0], w_mix.shape[1])
    chans = width // groups
    shape = (items, length // span, span, groups, chans)
    u_val = u_pre.astype(jnp.float32).reshape(shape)
    v_val = v_pre.astype(jnp.float32).reshape(shape)
    cotan = grad_s.astype(jnp.float32).reshape(shape)
    upper, u_back = jax.vjp(jax.nn.gelu, u_val)
    gated, v_back = jax.vjp(jax.nn.gelu, v_val)
    centre = gated - jnp.mean(gated, axis=-1, keepdims=True)
    inverse = lax.rsqrt(jnp.mean(centre * centre, axis=-1, keepdims=True) + EPS)
    scaled = centre * inverse
    normed = (scaled * gain + shift).astype(jnp.bfloat16)
    lower = jnp.tril(jnp.ones((span, span), dtype=bool))
    w_low = jnp.where(lower[None], w_mix, jnp.zeros_like(w_mix))
    mixed = jnp.einsum("gts,insgc->intgc", w_low, normed, preferred_element_type=jnp.float32)
    mixed = mixed + jnp.transpose(mix_bias)[:, :, None]
    gated_out = (upper * mixed).astype(jnp.bfloat16)
    d_mixed = cotan * upper
    d_mixed_b = d_mixed.astype(jnp.bfloat16)
    grad_u = u_back(cotan * mixed)[0].astype(jnp.bfloat16).reshape(items, length, width)
    grad_bias = jnp.transpose(jnp.sum(d_mixed, axis=(0, 1, 4)))
    grad_w = jnp.einsum("intgc,insgc->gts", d_mixed_b, normed, preferred_element_type=jnp.float32)
    grad_w = jnp.where(lower[None], grad_w, jnp.zeros_like(grad_w))
    d_normed = jnp.einsum("gts,intgc->insgc", w_low, d_mixed_b, preferred_element_type=jnp.float32)
    grad_gain = jnp.sum(d_normed * scaled, axis=(0, 1, 2))
    grad_shift = jnp.sum(d_normed, axis=(0, 1, 2))
    d_scaled = d_normed * gain
    d_gated = inverse * (
        d_scaled
        - jnp.mean(d_scaled, axis=-1, keepdims=True)
        - scaled * jnp.mean(d_scaled * scaled, axis=-1, keepdims=True)
    )
    grad_v = v_back(d_gated)[0].astype(jnp.bfloat16).reshape(items, length, width)
    return (
        grad_u,
        grad_v,
        gated_out.reshape(items, length, width),
        grad_w,
        grad_bias,
        grad_gain,
        grad_shift,
    )


def on_device(u_pre, v_pre, d_out, w_mix, mix_bias, norm_gain, norm_shift, w_out):
    grad_s = lax.dot_general(
        d_out,
        lax.all_gather(w_out, "dp", axis=0, tiled=True),
        (((2,), (1,)), ((), ())),
        preferred_element_type=jnp.float32,
    ).astype(jnp.bfloat16)
    grad_u, grad_v, gated_out, grad_w, grad_bias, grad_gain, grad_shift = mechanism(
        grad_s, u_pre, v_pre, w_mix, mix_bias, norm_gain, norm_shift
    )
    grad_w, grad_bias, grad_gain, grad_shift = lax.psum(
        (grad_w, grad_bias, grad_gain, grad_shift), ("sp", "dp")
    )
    width = gated_out.shape[2]
    flat_d = d_out.reshape(-1, d_out.shape[2])
    flat_s = gated_out.reshape(-1, width)
    num_sp = lax.axis_size("sp")
    num_dp = lax.axis_size("dp")
    piece_rows = width // (num_sp * num_dp)
    reordered = (
        flat_s.reshape(-1, num_dp, num_sp, piece_rows).transpose(0, 2, 1, 3).reshape(-1, width)
    )
    summed = lax.psum_scatter(
        lax.dot_general(
            reordered, flat_d, (((0,), (0,)), ((), ())), preferred_element_type=jnp.float32
        ),
        ("sp", "dp"),
        scatter_dimension=0,
        tiled=True,
    )
    grad_w_out = lax.all_gather(summed, "sp", axis=0, tiled=True)
    return (grad_u, grad_v, grad_w_out, grad_w, grad_bias, grad_gain, grad_shift)


def solution(mesh):
    return jax.shard_map(
        on_device,
        mesh=mesh,
        in_specs=(
            P("dp", "sp", None),
            P("dp", "sp", None),
            P("dp", "sp", None),
            P(),
            P(),
            P(),
            P(),
            P("dp", None),
        ),
        out_specs=(P("dp", "sp", None), P("dp", "sp", None), P("dp", None), P(), P(), P(), P()),
        check_vma=False,
    )
```

profile of v0, /device:TPU:27, one launch (start us, length us, event | category | flops | bytes accessed | tf_op | source)
XLA Modules:
  0.0 542.0 jit_solution(12029540268014962513)
XLA Ops:
  7.9 3.2 convert_bitcast_fusion
  11.2 5.2 copy.68
  16.4 9.7 %copy.45 = f32[1,8,128,16,128]{2,4,1,3,0:T(8,128)} copy(f32[1,8,128,16,128]{4,3,0,2,1:T(8,128)} %bitcast.90) | data formatting | bytes 16777216 | tf_op jit(solution)/shard_map/reshape | solution.py:14
  26.1 3.3 convert_bitcast_fusion.1
  29.4 5.2 copy.66
  34.6 8.8 %copy.39 = f32[1,8,128,16,128]{2,4,1,3,0:T(8,128)} copy(f32[1,8,128,16,128]{4,3,0,2,1:T(8,128)} %bitcast.94) | data formatting | bytes 16777216 | tf_op jit(solution)/shard_map/reshape | solution.py:15
  43.5 5.9 %fusion.52 = f32[8,128,16]{1,0,2:T(8,128)S(1)} fusion(f32[1,8,128,16,128]{2,4,1,3,0:T(8,128)} %copy.39), kind=kLoop, calls=%fused_computation.77 | loop fusion | flops 18857984 | bytes 8454144 | tf_op jit(solution)/shard_map/reduce_sum | solution.py:19
  49.4 3.7 multiply_reduce_fusion.2
  53.2 6.5 %fusion.35 = bf16[8,128,16,128]{3,1,0,2:T(8,128)(2,1)} fusion(f32[8,128,16,128]{3,2,1,0:T(8,128)S(1)} %bitcast.95, f32[16,128]{1,0:T(8,128)S(1)} %copy-done.6, f32[16,128]{1,0:T(8,128)S(1)} %copy-done.5, f32[8,128,16]{1,0,2:T(8,128)S(1)} %add_rsqrt_fusion, f32[8,128,16]{1,0,2:T(8,128)S(1)} %broadcast_multiply_fusion.2), kind=kLoop, calls=%fused_computation.52 | loop fusion | flops 27262976 | bytes 12730368 | tf_op jit(solution)/shard_map/convert_element_type | solution.py:22
  59.7 8.6 %all-gather.3.cloned.1.call-done = bf16[2048,2048]{1,0:T(8,128)(2,1)} async-done(((bf16[512,2048]{1,0:T(8,128)(2,1)}), bf16[2048,2048]{1,0:T(8,128)(2,1)}) %all-gather.3.cloned.1.call-update) | async-done | bytes 8388624 | tf_op jit(solution)/shard_map/all_gather | solution.py:58
  68.3 12.7 %convert_bitcast_fusion.2 = f32[128,8,16,128]{3,1,2,0:T(8,128)S(1)} fusion(bf16[2048,2048]{1,0:T(8,128)(2,1)} %all-gather.3.cloned.1.call-done, bf16[1,1024,2048]{2,1,0:T(8,128)(2,1)} %param.10), kind=kOutput, calls=%fused_computation.51 | convolution fusion | flops 8594128896 | bytes 20971520 | tf_op jit(solution)/shard_map/dot_general | solution.py:56
  81.0 5.2 copy.65
  86.2 8.8 %copy.41 = f32[1,8,128,16,128]{2,4,1,3,0:T(8,128)} copy(f32[1,8,128,16,128]{4,3,2,1,0:T(8,128)} %bitcast.92) | data formatting | bytes 16777216 | tf_op jit(solution)/shard_map/reshape | solution.py:16
  95.0 14.1 %multiply_convert_fusion = (bf16[1,8,128,16,128]{2,4,1,3,0:T(8,128)(2,1)S(1)}, bf16[1,8,128,16,128]{2,4,1,3,0:T(8,128)(2,1)}, f32[128,16]{0,1:T(8,128)S(1)}) fusion(f32[128,16]{0,1:T(8,128)S(1)} %bitcast.99, f32[1,8,128,16,128]{2,4,1,3,0:T(8,128)} %copy.45, f32[1,8,128,16,128]{2,4,1,3,0:T(8,128)} %copy.41, bf16[8,128,16,128]{3,1,0,2:T(8,128)(2,1)} %fusion.35, ...), kind=kOutput, calls=%fused_computation.46 | convolution fusion | flops 593754112 | bytes 29917184 | tf_op jit(solution)/shard_map/gts,insgc->intgc/dot_general | solution.py:25
  109.1 5.6 %copy.58 = bf16[1,8,128,16,128]{2,1,4,3,0:T(8,128)(2,1)} copy(bf16[1,8,128,16,128]{2,4,1,3,0:T(8,128)(2,1)S(1)} %get-tuple-element.14) | data formatting | bytes 8388608 | tf_op jit(solution)/shard_map/convert_element_type | solution.py:27
  114.7 7.3 %reshape_reshape_reshape.3 = bf16[1024,4,8,64]{0,3,2,1:T(8,128)(2,1)} reshape(bf16[1,8,128,16,128]{2,1,4,3,0:T(8,128)(2,1)} %copy.58) | data formatting | bytes 8388608 | tf_op jit(solution)/shard_map/reshape;reshape;reshape | solution.py:75
  122.1 2.9 copy.59
  125.5 11.7 %fusion.37 = f32[2048,2048]{1,0:T(8,128)} fusion(bf16[1024,2048]{0,1:T(8,128)(2,1)S(1)} %bitcast.97, bf16[1,1024,2048]{2,1,0:T(8,128)(2,1)S(1)} %copy-done.7), kind=kOutput, calls=%fused_computation.57 | convolution fusion | flops 8589934592 | bytes 25165824 | tf_op jit(solution)/shard_map/dot_general | solution.py:78
  137.3 183.8 %reduce-scatter.2.cloned.1.call-done = f32[64,2048]{1,0:T(8,128)} async-done(((f32[2048,2048]{1,0:T(8,128)}), f32[64,2048]{1,0:T(8,128)}) %reduce-scatter.2.cloned.1.call-update) | async-done | bytes 524304 | tf_op jit(solution)/shard_map/reduce_scatter | solution.py:77
  321.2 10.4 %fusion.33 = bf16[8,128,16,128]{3,1,0,2:T(8,128)(2,1)S(1)} fusion(f32[8,128,16,128]{3,2,1,0:T(8,128)} %bitcast.93, f32[8,128,16,128]{3,2,1,0:T(8,128)} %bitcast.91), kind=kLoop, calls=%fused_computation.39 | loop fusion | flops 20971520 | bytes 20971520 | tf_op jit(solution)/shard_map/convert_element_type | solution.py:29
  331.6 2.0 copy-done.2
  333.6 2.2 fusion.43
  335.9 11.5 %fusion.34 = (f32[16,128]{1,0:T(8,128)S(1)}, f32[8,128,16]{1,0,2:T(8,128)S(1)}, f32[8,128,16]{1,0,2:T(8,128)S(1)}, f32[16,128]{1,0:T(8,128)S(1)}, f32[16,8,128,128]{3,2,1,0:T(8,128)}) fusion(f32[8,128,16]{1,0,2:T(8,128)S(1)} %add_rsqrt_fusion, f32[8,128,16]{1,0,2:T(8,128)S(1)} %broadcast_multiply_fusion.2, f32[1,8,128,16,128]{2,4,1,3,0:T(8,128)} %copy.39, ...), kind=kOutput, calls=%fused_computation.44 | convolution fusion | flops 572747776 | bytes 21798912 | tf_op jit(solution)/shard_map/gts,intgc->insgc/dot_general | solution.py:34
  347.4 12.2 %fusion.6 = bf16[1,8,128,16,128]{2,4,1,3,0:T(8,128)(2,1)} fusion(f32[1,8,128,16,128]{2,4,1,3,0:T(8,128)} %copy.39, f32[16,8,128,128]{3,2,1,0:T(8,128)} %get-tuple-element.17, f32[8,128,16]{1,0,2:T(8,128)S(1)} %get-tuple-element.18, f32[8,128,16]{1,0,2:T(8,128)S(1)} %get-tuple-element.19, f32[16,128]{1,0:T(8,128)S(1)} %copy-done.5, ...), kind=kLoop, calls=%fused_computation.12 | loop fusion | flops 58720256 | bytes 21241856 | tf_op jit(solution)/shard_map/convert_element_type | solution.py:43
  359.6 6.7 %copy.47 = bf16[1,8,128,16,128]{4,3,2,1,0:T(8,128)(2,1)} copy(bf16[1,8,128,16,128]{2,4,1,3,0:T(8,128)(2,1)} %get-tuple-element.15) | data formatting | bytes 8388608 | tf_op jit(solution)/shard_map/convert_element_type | solution.py:30
  366.3 7.3 %reshape.458 = bf16[1,1024,2048]{2,1,0:T(8,128)(2,1)} reshape(bf16[1,8,128,16,128]{4,3,2,1,0:T(8,128)(2,1)} %copy.47) | data formatting | bytes 8388608 | tf_op jit(solution)/shard_map/reshape | solution.py:30
  373.6 6.7 %copy.56 = bf16[1,8,128,16,128]{4,3,2,1,0:T(8,128)(2,1)} copy(bf16[1,8,128,16,128]{2,4,1,3,0:T(8,128)(2,1)} %fusion.6) | data formatting | bytes 8388608 | tf_op jit(solution)/shard_map/convert_element_type | solution.py:43
  380.3 7.3 %reshape.461 = bf16[1,1024,2048]{2,1,0:T(8,128)(2,1)} reshape(bf16[1,8,128,16,128]{4,3,2,1,0:T(8,128)(2,1)} %copy.56) | data formatting | bytes 8388608 | tf_op jit(solution)/shard_map/reshape | solution.py:43
  387.6 39.3 %all-reduce = (f32[16,128]{1,0:T(8,128)}, f32[16,128]{1,0:T(8,128)}, f32[16,128]{1,0:T(8,128)}) all-reduce(f32[16,128]{1,0:T(8,128)S(1)} %bitcast.98, f32[16,128]{1,0:T(8,128)S(1)} %get-tuple-element.7, f32[16,128]{1,0:T(8,128)S(1)} %get-tuple-element.10), channel_id=1, replica_groups=mesh['sp'=8,'dp'=4] {'sp','dp'}, use_global_device_ids=true, to_apply=%region_7.8 | all-reduce | flops 6144 | bytes 49152 | tf_op jit(solution)/shard_map/psum | solution.py:65
  426.9 102.6 %all-reduce.3.cloned.1.call-done = f32[16,128,128]{2,1,0:T(8,128)} async-done(((f32[16,128,128]{2,1,0:T(8,128)}), f32[16,128,128]{2,1,0:T(8,128)}) %all-reduce.3.cloned.1.call-update) | async-done | bytes 1048592 | tf_op jit(solution)/shard_map/psum | solution.py:65
  529.5 4.8 copy.78
  534.3 1.0 copy.79
  (32 shorter events, 1.6 us)
Async XLA Ops:
  7.2 61.1 %all-gather.3.cloned.1.call-start = ((), (), s32[]{:S(2)}) async-start(), calls=%async_computation.1 | async-start | bytes 10485760 | tf_op jit(solution)/shard_map/all_gather | solution.py:58
  7.9 313.2 %reduce-scatter.2.cloned.1.call-start = ((), (), s32[]{:S(2)}) async-start(), calls=%async_computation.2 | async-start | bytes 17301504 | tf_op jit(solution)/shard_map/reduce_scatter | solution.py:77
  43.4 5.9 %copy-start = (f32[1,8,128,16,128]{2,4,1,3,0:T(8,128)S(1)}, f32[1,8,128,16,128]{2,4,1,3,0:T(8,128)}, u32[]{:S(2)}) copy-start(f32[1,8,128,16,128]{2,4,1,3,0:T(8,128)} %copy.39) | copy-start | bytes 25165828
  43.5 9.7 %copy-start.1 = (f32[128,8,16,128]{3,2,1,0:T(8,128)S(1)}, f32[128,8,16,128]{3,2,1,0:T(8,128)}, u32[]{:S(2)}) copy-start(f32[128,8,16,128]{3,2,1,0:T(8,128)} %copy.66) | copy-start | bytes 25165828
  43.5 9.7 %copy-start.5 = (f32[16,128]{1,0:T(8,128)S(1)}, f32[16,128]{1,0:T(8,128)}, u32[]{:S(2)}) copy-start(f32[16,128]{1,0:T(8,128)} %param.13) | copy-start | bytes 24580
  43.5 9.7 %copy-start.6 = (f32[16,128]{1,0:T(8,128)S(1)}, f32[16,128]{1,0:T(8,128)}, u32[]{:S(2)}) copy-start(f32[16,128]{1,0:T(8,128)} %param.14) | copy-start | bytes 24580
  86.2 8.8 %copy-start.8 = (bf16[16,128,128]{2,1,0:T(8,128)(2,1)S(1)}, bf16[16,128,128]{2,1,0:T(8,128)(2,1)}, u32[]{:S(2)}) copy-start(bf16[16,128,128]{2,1,0:T(8,128)(2,1)} %param.11) | copy-start | bytes 1572868
  86.2 8.8 %copy-start.9 = (f32[16,128]{1,0:T(8,128)S(1)}, f32[16,128]{1,0:T(8,128)}, u32[]{:S(2)}) copy-start(f32[16,128]{1,0:T(8,128)} %param.12) | copy-start | bytes 24580
  122.1 3.4 copy-start.7
  137.2 289.7 %all-gather.5.cloned.1.call-start = ((), (), s32[]{:S(2)}) async-start(), calls=%async_computation.3 | async-start | bytes 4718592 | tf_op jit(solution)/shard_map/all_gather | solution.py:85
  321.1 208.4 %all-reduce.3.cloned.1.call-start = ((), (), s32[]{:S(2)}) async-start(), calls=%async_computation.4 | async-start | bytes 2097152 | tf_op jit(solution)/shard_map/psum | solution.py:65
  321.2 12.5 %copy-start.3 = (bf16[8,128,16,128]{3,1,0,2:T(8,128)(2,1)S(1)}, bf16[8,128,16,128]{3,1,0,2:T(8,128)(2,1)}, u32[]{:S(2)}) copy-start(bf16[8,128,16,128]{3,1,0,2:T(8,128)(2,1)} %fusion.35) | copy-start | bytes 12582916
  331.6 2.0 copy-start.2
  529.5 4.8 copy-start.4
Sparse Core Ops, SparseCore 0:
  9.5 58.7 all-gather.2
  137.3 183.7 reduce-scatter.1
  323.2 72.5 all-gather.4
  401.5 127.9 all-reduce.2
where the time goes:
time: 551 us; the launch traced here: 542 us
  waiting for transfers between devices  296 us (54%)
  local copies, waits for them, and re-layouts  95.1 us (17%)
  matrix products  52.2 us (9%)
  other arithmetic  45.3 us (8%)
  blocking collectives  39.3 us (7%)
  between operations  14.2 us (3%)
    reduce_scatter x1, waiting for transfers between devices, on_device(): lax.psum_scatter(lax.dot_general(reordered, flat_d, (((0,), (0,)), ((), (...  184 us
    psum x1, waiting for transfers between devices, on_device(): lax.psum((grad_w, grad_bias, grad_gain, grad_shift), ('sp', 'dp'))  103 us
    psum x1, blocking collectives, on_device(): lax.psum((grad_w, grad_bias, grad_gain, grad_shift), ('sp', 'dp'))  39.3 us
    unnamed x25, local copies, waits for them, and re-layouts  24 us
    dot_general x1, matrix products, mechanism(): jnp.einsum('gts,insgc->intgc', w_low, normed, preferred_element_type=jnp....  14.1 us
    dot_general x1, matrix products, on_device(): lax.dot_general(d_out, lax.all_gather(w_out, 'dp', axis=0, tiled=True), (...  12.7 us
    convert_element_type x1, other arithmetic, mechanism(): v_back(d_gated)[0].astype(jnp.bfloat16).reshape(items, length, width)  12.2 us
    dot_general x1, matrix products, on_device(): lax.dot_general(reordered, flat_d, (((0,), (0,)), ((), ())), preferred_el...  11.7 us
  transfers between devices with their start and end apart: 4, of which 3 were waited for; matrix products, arithmetic and copies ran while one was open for 21% of the time, Pallas kernels for 0%

commit v1 on v0

v1 whole, which is shorter than its diff:
```python
import functools

import jax
import jax.numpy as jnp
from jax import lax
from jax.experimental import pallas as pl
from jax.experimental.pallas import tpu as pltpu
from jax.sharding import PartitionSpec as P

EPS = 1e-05
K0 = 0.7978845608028654
K1 = 0.044715
F32 = jnp.float32
BF16 = jnp.bfloat16


def gelu_parts(a):
    sq = a * a
    t = jnp.tanh(a * (K0 + (K0 * K1) * sq))
    half = 0.5 * (1.0 + t)
    return sq, t, half


def gelu(a):
    _, _, half = gelu_parts(a)
    return a * half


def gelu_both(a):
    sq, t, half = gelu_parts(a)
    slope = half + (0.5 * a) * (1.0 - t * t) * (K0 + (3.0 * K0 * K1) * sq)
    return a * half, slope


def norm_parts(gated):
    centre = gated - jnp.mean(gated, axis=-1, keepdims=True)
    inverse = lax.rsqrt(jnp.mean(centre * centre, axis=-1, keepdims=True) + EPS)
    return centre * inverse, inverse


def mm(a, b, ca, cb):
    return lax.dot_general(a, b, (((ca,), (cb,)), ((), ())), preferred_element_type=F32)


def kernel(
    dims,
    u_ref, v_ref, d_ref, wmix_ref, bias_ref, gain_ref, shift_ref, w_ref,
    gu_ref, gv_ref, dw_ref, sm_ref,
    wfull, part, rcore, rx, rsp, ag, gs, got, wl_ref, wlt_ref, acc, sbuf, srecv,
    wown_s, wown_r, wx_s, wx_r, wsp_s, wsp_r, wfw_s, wfw_r,
    core_s, core_r, xs_s, xs_r, rs_s, rs_r, ag_s, ag_r,
    s1_s, s1_r, s2_s, s2_r,
):
    n_sp, n_dp, gpc, span, chans, width, rows = dims
    pairs = n_dp // 2
    n_dev = n_sp * n_dp
    nb = rows // span
    s = lax.axis_index("sp")
    dpi = lax.axis_index("dp")
    x = dpi // 2
    c = dpi % 2
    other = 1 - c
    mate = {"sp": s, "dp": 2 * x + other}
    part_rows = span // (n_dev // (n_dp * gpc))

    def rc(src, dst, ssem, rsem, dev):
        return pltpu.make_async_remote_copy(
            src_ref=src, dst_ref=dst, send_sem=ssem, recv_sem=rsem,
            device_id=dev, device_id_type=pl.DeviceIdType.MESH,
        )

    def each(lo, hi, fn):
        def body(i, carry):
            fn(i)
            return carry
        lax.fori_loop(lo, hi, body, 0)

    def up(k):
        return (x + k) % pairs

    def down(k):
        return (x + pairs - k) % pairs

    def w_own():
        return rc(w_ref, wfull.at[dpi], wown_s, wown_r, mate)

    def w_x(k):
        return rc(w_ref.at[s], wfull.at[dpi, s], wx_s.at[k], wx_r.at[k], {"sp": s, "dp": 2 * up(k) + c})

    def w_sp(k, o):
        src = 2 * down(k) + c
        return rc(wfull.at[src, s], wfull.at[src, s], wsp_s.at[k, o], wsp_r.at[k, o], {"sp": (s + o) % n_sp, "dp": dpi})

    def w_fw(k):
        src = 2 * down(k) + c
        return rc(wfull.at[src], wfull.at[src], wfw_s.at[k], wfw_r.at[k], mate)

    def gid(xx, cc, q):
        return (2 * xx + cc) * gpc + q

    def t_core(k, q):
        return rc(part.at[gid(up(k), other, q)], rcore.at[k, q], core_s.at[k, q], core_r.at[k, q], mate)

    def t_x(k, q):
        return rc(part.at[gid(up(k), c, q)], rx.at[k, q], xs_s.at[k, q], xs_r.at[k, q], {"sp": s, "dp": 2 * up(k) + c})

    def t_rs(q, o):
        to = (s + o) % n_sp
        return rc(part.at[gid(x, c, q), to], rsp.at[q, o], rs_s.at[q, o], rs_r.at[q, o], {"sp": to, "dp": dpi})

    def t_ag(q, o):
        to = (s + o) % n_sp
        return rc(ag.at[q, s], ag.at[q, s], ag_s.at[q, o], ag_r.at[q, o], {"sp": to, "dp": dpi})

    me = s * n_dp + dpi

    def t_s1(o):
        to = (me + o) % n_dev
        return rc(sbuf.at[to], srecv.at[o], s1_s.at[o], s1_r.at[o], {"sp": to // n_dp, "dp": to % n_dp})

    def t_s2(o):
        to = (me + o) % n_dev
        return rc(sbuf.at[me], srecv.at[n_dev + me], s2_s.at[o], s2_r.at[o], {"sp": to // n_dp, "dp": to % n_dp})

    row = lax.broadcasted_iota(jnp.int32, (span, span), 0)
    col = lax.broadcasted_iota(jnp.int32, (span, span), 1)
    lower = row >= col

    w_own().start()
    for k in range(1, pairs):
        w_x(k).start()
    wfull[dpi] = w_ref[...]

    def lanes(g):
        return pl.ds(pl.multiple_of(g * chans, chans), chans)

    def forward_group(g, half):
        wl = jnp.where(lower, wmix_ref[g], jnp.zeros((), BF16))
        bias = bias_ref[g]
        gain = gain_ref[g]
        shift = shift_ref[g]
        for b in range(nb):
            at = pl.ds(b * span, span)
            scaled, _ = norm_parts(gelu(v_ref[at, lanes(g)].astype(F32)))
            normed = (scaled * gain + shift).astype(BF16)
            mixed = mm(wl, normed, 1, 0) + bias
            out = (gelu(u_ref[at, lanes(g)].astype(F32)) * mixed).astype(BF16)
            got[pl.ds(pl.multiple_of(half * span, span), span), pl.ds(b * span, span)] = out.T

    def core_sum(k, q):
        t_core(k, q).wait_recv()
        g = gid(up(k), c, q)

        def one(j):
            part[g, j] = (part[g, j].astype(F32) + rcore[k, q, j].astype(F32)).astype(BF16)
        each(0, n_sp, one)
        t_x(k, q).start()

    def forward_step(i):
        k = (i // gpc + 1) % pairs
        q = i % gpc
        keep = gid(up(k), c, q)
        give = gid(up(k), other, q)
        each(0, 2, lambda h: forward_group(gid(up(k), (c + h) % 2, q), h))

        def one(j):
            r = mm(got[...], d_ref[:, pl.ds(pl.multiple_of(j * width, width), width)], 1, 0)
            part[keep, j] = r[:span].astype(BF16)
            part[give, j] = r[span:].astype(BF16)
        each(0, n_sp, one)
        t_core(k, q).start()
        last = i - 1

        @pl.when((i > 0) & (last < (pairs - 1) * gpc))
        def _():
            core_sum((last // gpc + 1) % pairs, last % gpc)

    n_far = (pairs - 1) * gpc
    each(0, n_far, forward_step)
    for k in range(1, pairs):
        w_x(k).wait_recv()
        each(1, n_sp, lambda o: w_sp(k, o).start())
    each(n_far, n_far + gpc, forward_step)
    w_own().wait_recv()

    def forward_w():
        for k in range(1, pairs):
            each(1, n_sp, lambda o: w_sp(k, o).wait_recv())
            w_fw(k).start()

    def rs_start(q):
        t_core(0, q).wait_recv()
        for k in range(1, pairs):
            t_x(k, q).wait_recv()
        g = gid(x, c, q)

        def one(j):
            total = part[g, j].astype(F32) + rcore[0, q, j].astype(F32)
            for k in range(1, pairs):
                total = total + rx[k, q, j].astype(F32)
            part[g, j] = total.astype(BF16)
        each(0, n_sp, one)
        each(1, n_sp, lambda o: t_rs(q, o).start())

    def ag_start(q):
        each(1, n_sp, lambda o: t_rs(q, o).wait_recv())
        total = part[gid(x, c, q), s].astype(F32)
        for o in range(1, n_sp):
            total = total + rsp[q, o].astype(F32)
        ag[q, s] = total.astype(BF16)
        each(1, n_sp, lambda o: t_ag(q, o).start())

    sbuf[...] = jnp.zeros_like(sbuf)

    def backward_group(g, half):
        wl = jnp.where(lower, wmix_ref[g], jnp.zeros((), BF16))
        wlt = wl.T
        bias = bias_ref[g]
        gain = gain_ref[g]
        shift = shift_ref[g]
        acc[...] = jnp.zeros_like(acc)
        wl_ref[...] = wl
        wlt_ref[...] = wlt
        hl = pl.ds(pl.multiple_of(half * chans, chans), chans)
        for b in range(nb):
            at = pl.ds(b * span, span)
            gated, v_slope = gelu_both(v_ref[at, lanes(g)].astype(F32))
            scaled, inverse = norm_parts(gated)
            normed = (scaled * gain + shift).astype(BF16)
            mixed = mm(wl_ref[...], normed, 1, 0) + bias
            upper, u_slope = gelu_both(u_ref[at, lanes(g)].astype(F32))
            cot = gs[at, hl].astype(F32)
            dm = cot * upper
            dmb = dm.astype(BF16)
            gu_ref[at, lanes(g)] = (cot * mixed * u_slope).astype(BF16)
            acc[0] += dm
            acc[1] += mm(dmb, normed, 1, 1)
            dn = mm(wlt_ref[...], dmb, 1, 0)
            acc[2] += dn * scaled
            acc[3] += dn
            e = dn * gain
            m1 = jnp.mean(e, axis=-1, keepdims=True)
            m2 = jnp.mean(e * scaled, axis=-1, keepdims=True)
            gv_ref[at, lanes(g)] = (v_slope * (inverse * (e - m1 - scaled * m2))).astype(BF16)
        grad_w = jnp.where(lower, acc[1], 0.0)
        per = span // part_rows
        for p in range(per):
            sbuf[g * per + p, 0:part_rows, :] = grad_w[p * part_rows : (p + 1) * part_rows].astype(BF16)
        g_bias = jnp.sum(acc[0].T, axis=0, keepdims=True)
        g_gain = jnp.sum(acc[2], axis=0, keepdims=True)
        g_shift = jnp.sum(acc[3], axis=0, keepdims=True)
        r16 = lax.broadcasted_iota(jnp.int32, (16, chans), 0)
        extra = jnp.where(r16 == 0, g_bias, jnp.where(r16 == 1, g_gain, jnp.where(r16 == 2, g_shift, 0.0)))
        sbuf[g * per, part_rows : part_rows + 16, :] = extra.astype(BF16)

    per_chunk = gpc // 2
    rs_rows = wfull.shape[2]

    def backward_step(i):
        turn = i // per_chunk
        k = turn // 2
        chunk = 2 * down(k) + (c + turn) % 2
        two = i % per_chunk
        first = 2 * span // rs_rows
        wrows = wfull[chunk, pl.ds(two * first, first)].reshape(2 * span, wfull.shape[3])

        def one(j):
            at = pl.ds(pl.multiple_of(j * 2 * span, 2 * span), 2 * span)
            gs[at, :] = mm(d_ref[at, :], wrows, 1, 1).astype(BF16)
        each(0, rows // (2 * span), one)
        each(0, 2, lambda h: backward_group(chunk * gpc + 2 * two + h, h))

    n_steps = n_dp * per_chunk
    actions = {}

    def put(step, fn):
        actions.setdefault(min(step, n_steps - 1), []).append(fn)

    put(0, forward_w)
    for q in range(gpc):
        put(2 * per_chunk - 2 + (q * n_steps) // (2 * gpc) + q // 2, functools.partial(rs_start, q))
        put(2 * per_chunk - 1 + (q * n_steps) // (2 * gpc) + q // 2, functools.partial(ag_start, q))
    for k in range(1, pairs):
        put(2 * per_chunk * k - 1, lambda k=k: None)

    def whole_step(i):
        turn = i // per_chunk
        for k in range(1, pairs):
            @pl.when(i == (2 * k + 1) * per_chunk)
            def _(k=k):
                w_fw(k).wait_recv()
        backward_step(i)
        for step in sorted(actions):
            @pl.when(i == step)
            def _(step=step):
                for fn in actions[step]:
                    fn()

    core_sum_last = n_far - 1
    del core_sum_last
    each(0, n_steps, whole_step)

    each(1, n_dev, lambda o: t_s1(o).start())
    each(1, n_dev, lambda o: t_s1(o).wait_recv())
    acc_s = sbuf[me].astype(F32)
    acc_s = lax.fori_loop(1, n_dev, lambda o, a: a + srecv[o].astype(F32), acc_s)
    each(1, n_dev, lambda o: t_s1(o).wait_send())
    sbuf[me] = acc_s.astype(BF16)
    srecv[n_dev + me] = acc_s.astype(BF16)
    each(1, n_dev, lambda o: t_s2(o).start())

    for q in range(gpc):
        each(1, n_sp, lambda o: t_ag(q, o).wait_recv())
        for j in range(n_sp):
            dw_ref[q * span : (q + 1) * span, j * width : (j + 1) * width] = ag[q, j]

    each(1, n_dev, lambda o: t_s2(o).wait_recv())
    sm_ref[...] = srecv[n_dev : 2 * n_dev]

    w_own().wait_send()
    for k in range(1, pairs):
        w_x(k).wait_send()
        each(1, n_sp, lambda o: w_sp(k, o).wait_send())
        w_fw(k).wait_send()
        each(0, gpc, lambda q: t_x(k, q).wait_send())
    for k in range(pairs):
        each(0, gpc, lambda q: t_core(k, q).wait_send())
    for q in range(gpc):
        each(1, n_sp, lambda o: t_rs(q, o).wait_send())
        each(1, n_sp, lambda o: t_ag(q, o).wait_send())
    each(1, n_dev, lambda o: t_s2(o).wait_send())


def on_device(n_sp, n_dp, u_pre, v_pre, d_out, w_mix, mix_bias, norm_gain, norm_shift, w_out):
    _, rows, wide = u_pre.shape
    depth = d_out.shape[2]
    groups, span = w_mix.shape[:2]
    chans = wide // groups
    gpc = groups // n_dp
    width = depth // n_sp
    n_dev = n_sp * n_dp
    per = n_dev // groups
    part_rows = span // per
    shard = w_out.shape[0]
    pairs = n_dp // 2
    dims = (n_sp, n_dp, gpc, span, chans, width, rows)
    dma = pltpu.SemaphoreType.DMA
    vm = pltpu.VMEM
    piece = (n_sp, span, width)
    scratch = [
        vm((n_dp, n_sp, shard // n_sp, depth), BF16),
        vm((groups,) + piece, BF16),
        vm((pairs, gpc) + piece, BF16),
        vm((pairs, gpc) + piece, BF16),
        vm((gpc,) + piece, BF16),
        vm((gpc,) + piece, BF16),
        vm((rows, 2 * chans), BF16),
        vm((2 * chans, rows), BF16),
        vm((span, span), BF16),
        vm((span, span), BF16),
        vm((4, span, chans), F32),
        vm((n_dev, part_rows + 16, chans), BF16),
        vm((2 * n_dev, part_rows + 16, chans), BF16),
        dma, dma,
        dma((pairs,)), dma((pairs,)),
        dma((pairs, n_sp)), dma((pairs, n_sp)),
        dma((pairs,)), dma((pairs,)),
        dma((pairs, gpc)), dma((pairs, gpc)),
        dma((pairs, gpc)), dma((pairs, gpc)),
        dma((gpc, n_sp)), dma((gpc, n_sp)),
        dma((gpc, n_sp)), dma((gpc, n_sp)),
        dma((n_dev,)), dma((n_dev,)),
        dma((n_dev,)), dma((n_dev,)),
    ]
    spec = pl.BlockSpec(memory_space=pltpu.VMEM)
    gu, gv, dw, sm = pl.pallas_call(
        functools.partial(kernel, dims),
        out_shape=(
            jax.ShapeDtypeStruct((rows, wide), BF16),
            jax.ShapeDtypeStruct((rows, wide), BF16),
            jax.ShapeDtypeStruct((shard, depth), BF16),
            jax.ShapeDtypeStruct((n_dev, part_rows + 16, chans), BF16),
        ),
        in_specs=[spec] * 8,
        out_specs=(spec,) * 4,
        scratch_shapes=scratch,
        compiler_params=pltpu.CompilerParams(has_side_effects=True, vmem_limit_bytes=67043328),
    )(
        u_pre[0], v_pre[0], d_out[0], w_mix,
        jnp.broadcast_to(mix_bias[:, :, None], (groups, span, chans)),
        norm_gain[:, None, :], norm_shift[:, None, :],
        w_out.reshape(n_sp, shard // n_sp, depth),
    )
    grad_w = sm[:, :part_rows].reshape(groups, span, span).astype(F32)
    extra = sm.reshape(groups, per, part_rows + 16, chans)[:, 0, part_rows:].astype(F32)
    return (gu[None], gv[None], dw.astype(F32), grad_w, extra[:, 0], extra[:, 1], extra[:, 2])


def solution(mesh):
    body = functools.partial(on_device, mesh.shape["sp"], mesh.shape["dp"])
    return jax.shard_map(
        body,
        mesh=mesh,
        in_specs=(
            P("dp", "sp", None),
            P("dp", "sp", None),
            P("dp", "sp", None),
            P(),
            P(),
            P(),
            P(),
            P("dp", None),
        ),
        out_specs=(P("dp", "sp", None), P("dp", "sp", None), P("dp", None), P(), P(), P(), P()),
        check_vma=False,
    )
```

time: 551 us -> 237 us (0.43); the launches traced: 542 us -> 236 us
  waiting for transfers between devices: 296 us -> 0 us
  Pallas kernels: 0 us -> 221 us
  local copies, waits for them, and re-layouts: 95.1 us -> 8.39 us
  matrix products: 52.2 us -> 0 us
  other arithmetic: 45.3 us -> 5.37 us
  blocking collectives: 39.3 us -> 0 us
  between operations: 14.2 us -> 0.67 us
    pallas_call x0 -> x1, Pallas kernels: none -> 221 us  [on_device(): pl.pallas_call(functools.partial(kernel, dims), out_shape=(jax.ShapeDtype...]
    reduce_scatter x1 -> x0, waiting for transfers between devices: 184 us -> none  [on_device(): lax.psum_scatter(lax.dot_general(reordered, flat_d, (((0,), (0,)), ((), (...]
    psum x1 -> x0, waiting for transfers between devices: 103 us -> none  [on_device(): lax.psum((grad_w, grad_bias, grad_gain, grad_shift), ('sp', 'dp'))]
    dot_general x5 -> x0, matrix products: 52.2 us -> none  [the longest x1 14.1 us: mechanism(): jnp.einsum('gts,insgc->intgc', w_low, normed, preferred_element_type=jnp....]
    reshape x5 -> x0, local copies, waits for them, and re-layouts: 41.9 us -> none  [the longest x1 9.73 us: mechanism(): u_val = u_pre.astype(jnp.float32).reshape(shape)]
    psum x1 -> x0, blocking collectives: 39.3 us -> none  [on_device(): lax.psum((grad_w, grad_bias, grad_gain, grad_shift), ('sp', 'dp'))]
    convert_element_type x3, other arithmetic: 29.1 us -> 5.37 us  [the longest x1 4.28 us: on_device(): dw.astype(F32)]
    convert_element_type x3 -> x0, local copies, waits for them, and re-layouts: 19 us -> none  [the longest x1 6.71 us: mechanism(): u_back(cotan * mixed)[0].astype(jnp.bfloat16).reshape(items, length, width)]
  transfers between devices with their start and end apart: 4 -> 0, of which waited for: 3 -> 0; matrix products, arithmetic and copies ran while one was open for 21% -> 0% of each run, Pallas kernels for 0% -> 0%
where the time goes in v1:
time: 237 us; the launch traced here: 236 us
  Pallas kernels  221 us (93%)
  local copies, waits for them, and re-layouts  8.39 us (4%)
  other arithmetic  5.37 us (2%)
    pallas_call x1, Pallas kernels, on_device(): pl.pallas_call(functools.partial(kernel, dims), out_shape=(jax.ShapeDtype...  221 us
    unnamed x8, local copies, waits for them, and re-layouts  5.72 us

profile of v1, /device:TPU:27, one launch (start us, length us, event | category | flops | bytes accessed | tf_op | source)
XLA Modules:
  0.0 235.7 jit_solution(11037856515353623227)
XLA Ops:
  0.6 2.0 broadcast_in_dim.18.bias_ref
  2.6 221.3 %shard_map.135 = (bf16[1024,2048]{1,0:T(8,128)(2,1)}, bf16[1024,2048]{1,0:T(8,128)(2,1)}, bf16[512,2048]{1,0:T(8,128)(2,1)}, bf16[32,80,128]{2,1,0:T(8,128)(2,1)}) custom-call(bf16[1024,2048]{1,0:T(8,128)(2,1)} %bitcast.24, bf16[1024,2048]{1,0:T(8,128)(2,1)} %bitcast.25, bf16[1024,2048]{1,0:T(8,128)(2,1)} %bitcast.26, bf16[16,128,128]{2,1,0:T(8,128)(2,1)} %wmix_ref.1, ...), custom_call_target="tpu_custom_call" | custom-call | tf_op jit(solution)/shard_map/pallas_call | solution.py:376
  223.9 0.0 copy-start.2
  223.9 0.0 copy-start.1
  224.0 4.3 %convert_element_type.15 = f32[512,2048]{1,0:T(8,128)} convert(bf16[512,2048]{1,0:T(8,128)(2,1)} %get-tuple-element.13) | non-fusion elementwise | flops 1048576 | bytes 6291456 | tf_op jit(solution)/shard_map/convert_element_type | solution.py:396
  228.2 0.0 copy-done.2
  228.2 0.1 slice.15
  228.3 1.1 bitcast_convert_fusion
  229.4 0.6 slice_bitcast_fusion
  230.0 0.0 copy-done.1
  230.0 0.0 copy-start
  230.0 2.1 copy.22
  232.1 1.6 copy-done
  233.7 2.0 copy.23
  (2 shorter events, 0.0 us)
Async XLA Ops:
  223.9 4.3 %copy-start.2 = (bf16[32,80,128]{2,1,0:T(8,128)(2,1)S(1)}, bf16[32,80,128]{2,1,0:T(8,128)(2,1)}, u32[]{:S(2)}) copy-start(bf16[32,80,128]{2,1,0:T(8,128)(2,1)} %get-tuple-element.14) | copy-start | bytes 1966084
  223.9 6.1 %copy-start.1 = (bf16[1024,2048]{1,0:T(8,128)(2,1)S(1)}, bf16[1024,2048]{1,0:T(8,128)(2,1)}, u32[]{:S(2)}) copy-start(bf16[1024,2048]{1,0:T(8,128)(2,1)} %get-tuple-element.11) | copy-start | bytes 12582916
  230.0 3.7 %copy-start = (bf16[1024,2048]{1,0:T(8,128)(2,1)S(1)}, bf16[1024,2048]{1,0:T(8,128)(2,1)}, u32[]{:S(2)}) copy-start(bf16[1024,2048]{1,0:T(8,128)(2,1)} %get-tuple-element.12) | copy-start | bytes 12582916

commit v2 on v1

--- a/solution.py
+++ b/solution.py
@@ -46,12 +46,13 @@
     dims,
     u_ref, v_ref, d_ref, wmix_ref, bias_ref, gain_ref, shift_ref, w_ref,
     gu_ref, gv_ref, dw_ref, sm_ref,
-    wfull, part, rcore, rx, rsp, ag, gs, got, wl_ref, wlt_ref, acc, sbuf, srecv,
-    wown_s, wown_r, wx_s, wx_r, wsp_s, wsp_r, wfw_s, wfw_r,
-    core_s, core_r, xs_s, xs_r, rs_s, rs_r, ag_s, ag_r,
+    wfull, part, rcore, rx, ry, rz, ag, gs, got, wl_ref, wlt_ref, acc, sbuf, srecv,
+    wown_s, wown_r, wx_s, wx_r, wz_s, wz_r, wy_s, wy_r, wfw_s, wfw_r,
+    core_s, core_r, xs_s, xs_r, yr_s, yr_r, zr_s, zr_r, za_s, za_r, ya_s, ya_r,
     s1_s, s1_r, s2_s, s2_r,
 ):
-    n_sp, n_dp, gpc, span, chans, width, rows = dims
+    n_y, n_z, n_dp, gpc, span, chans, width, rows = dims
+    n_sp = n_y * n_z
     pairs = n_dp // 2
     n_dev = n_sp * n_dp
     nb = rows // span
@@ -59,6 +60,9 @@
     dpi = lax.axis_index("dp")
     x = dpi // 2
     c = dpi % 2
+    y = s % n_y
+    z = s // n_y
+    zp = z % 2
     other = 1 - c
     mate = {"sp": s, "dp": 2 * x + other}
     part_rows = span // (n_dev // (n_dp * gpc))
@@ -84,12 +88,24 @@
     def w_own():
         return rc(w_ref, wfull.at[dpi], wown_s, wown_r, mate)
 
+    def at_y(o):
+        return {"sp": z * n_y + (y + o) % n_y, "dp": dpi}
+
+    def at_z(o):
+        return {"sp": (z + o) % n_z * n_y + y, "dp": dpi}
+
     def w_x(k):
-        return rc(w_ref.at[s], wfull.at[dpi, s], wx_s.at[k], wx_r.at[k], {"sp": s, "dp": 2 * up(k) + c})
-
-    def w_sp(k, o):
+        return rc(w_ref.at[y, zp], wfull.at[dpi, y, zp], wx_s.at[k], wx_r.at[k], {"sp": s, "dp": 2 * up(k) + c})
+
+    def w_z(k):
         src = 2 * down(k) + c
-        return rc(wfull.at[src, s], wfull.at[src, s], wsp_s.at[k, o], wsp_r.at[k, o], {"sp": (s + o) % n_sp, "dp": dpi})
+        to = {"sp": (z + 1 - 2 * zp) * n_y + y, "dp": dpi}
+        return rc(wfull.at[src, y, zp], wfull.at[src, y, zp], wz_s.at[k], wz_r.at[k], to)
+
+    def w_y(k, h, o):
+        src = 2 * down(k) + c
+        block = wfull.at[src, y, (zp + h) % 2]
+        return rc(block, block, wy_s.at[k, (zp + h) % 2, o], wy_r.at[k, (zp + h) % 2, o], at_y(o))
 
     def w_fw(k):
         src = 2 * down(k) + c
@@ -104,13 +120,17 @@
     def t_x(k, q):
         return rc(part.at[gid(up(k), c, q)], rx.at[k, q], xs_s.at[k, q], xs_r.at[k, q], {"sp": s, "dp": 2 * up(k) + c})
 
-    def t_rs(q, o):
-        to = (s + o) % n_sp
-        return rc(part.at[gid(x, c, q), to], rsp.at[q, o], rs_s.at[q, o], rs_r.at[q, o], {"sp": to, "dp": dpi})
-
-    def t_ag(q, o):
-        to = (s + o) % n_sp
-        return rc(ag.at[q, s], ag.at[q, s], ag_s.at[q, o], ag_r.at[q, o], {"sp": to, "dp": dpi})
+    def t_yr(q, o):
+        return rc(part.at[gid(x, c, q), (y + o) % n_y], ry.at[q, o], yr_s.at[q, o], yr_r.at[q, o], at_y(o))
+
+    def t_zr(q, o):
+        return rc(part.at[gid(x, c, q), y, (z + o) % n_z], rz.at[q, o], zr_s.at[q, o], zr_r.at[q, o], at_z(o))
+
+    def t_za(q, o):
+        return rc(ag.at[q, y, z], ag.at[q, y, z], za_s.at[q, o], za_r.at[q, o], at_z(o))
+
+    def t_ya(q, o):
+        return rc(ag.at[q, y], ag.at[q, y], ya_s.at[q, o], ya_r.at[q, o], at_y(o))
 
     me = s * n_dp + dpi
 
@@ -152,7 +172,8 @@
         g = gid(up(k), c, q)
 
         def one(j):
-            part[g, j] = (part[g, j].astype(F32) + rcore[k, q, j].astype(F32)).astype(BF16)
+            a, b = j // n_z, j % n_z
+            part[g, a, b] = (part[g, a, b].astype(F32) + rcore[k, q, a, b].astype(F32)).astype(BF16)
         each(0, n_sp, one)
         t_x(k, q).start()
 
@@ -165,8 +186,8 @@
 
         def one(j):
             r = mm(got[...], d_ref[:, pl.ds(pl.multiple_of(j * width, width), width)], 1, 0)
-            part[keep, j] = r[:span].astype(BF16)
-            part[give, j] = r[span:].astype(BF16)
+            part[keep, j // n_z, j % n_z] = r[:span].astype(BF16)
+            part[give, j // n_z, j % n_z] = r[span:].astype(BF16)
         each(0, n_sp, one)
         t_core(k, q).start()
         last = i - 1
@@ -176,39 +197,62 @@
             core_sum((last // gpc + 1) % pairs, last % gpc)
 
     n_far = (pairs - 1) * gpc
-    each(0, n_far, forward_step)
+    each(0, n_far // 2, forward_step)
     for k in range(1, pairs):
         w_x(k).wait_recv()
-        each(1, n_sp, lambda o: w_sp(k, o).start())
-    each(n_far, n_far + gpc, forward_step)
+        w_z(k).start()
+        each(1, n_y, lambda o: w_y(k, 0, o).start())
+    each(n_far // 2, n_far + 1, forward_step)
+    for k in range(1, pairs):
+        w_z(k).wait_recv()
+        each(1, n_y, lambda o: w_y(k, 1, o).start())
+    each(n_far + 1, n_far + gpc, forward_step)
     w_own().wait_recv()
 
     def forward_w():
         for k in range(1, pairs):
-            each(1, n_sp, lambda o: w_sp(k, o).wait_recv())
+            each(1, n_y, lambda o: w_y(k, 0, o).wait_recv())
+            each(1, n_y, lambda o: w_y(k, 1, o).wait_recv())
             w_fw(k).start()
 
-    def rs_start(q):
+    def yr_start(q):
         t_core(0, q).wait_recv()
         for k in range(1, pairs):
             t_x(k, q).wait_recv()
         g = gid(x, c, q)
 
         def one(j):
-            total = part[g, j].astype(F32) + rcore[0, q, j].astype(F32)
+            a, b = j // n_z, j % n_z
+            total = part[g, a, b].astype(F32) + rcore[0, q, a, b].astype(F32)
             for k in range(1, pairs):
-                total = total + rx[k, q, j].astype(F32)
-            part[g, j] = total.astype(BF16)
+                total = total + rx[k, q, a, b].astype(F32)
+            part[g, a, b] = total.astype(BF16)
         each(0, n_sp, one)
-        each(1, n_sp, lambda o: t_rs(q, o).start())
-
-    def ag_start(q):
-        each(1, n_sp, lambda o: t_rs(q, o).wait_recv())
-        total = part[gid(x, c, q), s].astype(F32)
-        for o in range(1, n_sp):
-            total = total + rsp[q, o].astype(F32)
-        ag[q, s] = total.astype(BF16)
-        each(1, n_sp, lambda o: t_ag(q, o).start())
+        each(1, n_y, lambda o: t_yr(q, o).start())
+
+    def zr_start(q):
+        each(1, n_y, lambda o: t_yr(q, o).wait_recv())
+        g = gid(x, c, q)
+
+        def one(b):
+            total = part[g, y, b].astype(F32)
+            for o in range(1, n_y):
+                total = total + ry[q, o, b].astype(F32)
+            part[g, y, b] = total.astype(BF16)
+        each(0, n_z, one)
+        each(1, n_z, lambda o: t_zr(q, o).start())
+
+    def za_start(q):
+        each(1, n_z, lambda o: t_zr(q, o).wait_recv())
+        total = part[gid(x, c, q), y, z].astype(F32)
+        for o in range(1, n_z):
+            total = total + rz[q, o].astype(F32)
+        ag[q, y, z] = total.astype(BF16)
+        each(1, n_z, lambda o: t_za(q, o).start())
+
+    def ya_start(q):
+        each(1, n_z, lambda o: t_za(q, o).wait_recv())
+        each(1, n_y, lambda o: t_ya(q, o).start())
 
     sbuf[...] = jnp.zeros_like(sbuf)
 
@@ -254,15 +298,14 @@
         sbuf[g * per, part_rows : part_rows + 16, :] = extra.astype(BF16)
 
     per_chunk = gpc // 2
-    rs_rows = wfull.shape[2]
+    flat = wfull.reshape(n_dp, wfull.shape[1] * 2 * wfull.shape[3], wfull.shape[4])
 
     def backward_step(i):
         turn = i // per_chunk
         k = turn // 2
         chunk = 2 * down(k) + (c + turn) % 2
         two = i % per_chunk
-        first = 2 * span // rs_rows
-        wrows = wfull[chunk, pl.ds(two * first, first)].reshape(2 * span, wfull.shape[3])
+        wrows = flat[chunk, pl.ds(pl.multiple_of(two * 2 * span, 2 * span), 2 * span), :]
 
         def one(j):
             at = pl.ds(pl.multiple_of(j * 2 * span, 2 * span), 2 * span)
@@ -276,12 +319,19 @@
     def put(step, fn):
         actions.setdefault(min(step, n_steps - 1), []).append(fn)
 
-    put(0, forward_w)
-    for q in range(gpc):
-        put(2 * per_chunk - 2 + (q * n_steps) // (2 * gpc) + q // 2, functools.partial(rs_start, q))
-        put(2 * per_chunk - 1 + (q * n_steps) // (2 * gpc) + q // 2, functools.partial(ag_start, q))
-    for k in range(1, pairs):
-        put(2 * per_chunk * k - 1, lambda k=k: None)
+    put(min(2, 2 * per_chunk - 2), forward_w)
+    when = ((-1, 1, 3, 5), (0, 2, 4, 6), (2, 4, 6, 8), (4, 6, 8, 9))
+    late = []
+    stages = (yr_start, zr_start, za_start, ya_start)
+    plan = [(when[q % 4][n], n, q) for q in range(gpc) for n in range(4)]
+    for step, n, q in sorted(plan):
+        fn = functools.partial(stages[n], q)
+        if step < 0:
+            fn()
+        elif step < n_steps:
+            put(step, fn)
+        else:
+            late.append(fn)
 
     def whole_step(i):
         turn = i // per_chunk
@@ -296,11 +346,11 @@
                 for fn in actions[step]:
                     fn()
 
-    core_sum_last = n_far - 1
-    del core_sum_last
     each(0, n_steps, whole_step)
 
     each(1, n_dev, lambda o: t_s1(o).start())
+    for fn in late:
+        fn()
     each(1, n_dev, lambda o: t_s1(o).wait_recv())
     acc_s = sbuf[me].astype(F32)
     acc_s = lax.fori_loop(1, n_dev, lambda o, a: a + srecv[o].astype(F32), acc_s)
@@ -310,9 +360,9 @@
     each(1, n_dev, lambda o: t_s2(o).start())
 
     for q in range(gpc):
-        each(1, n_sp, lambda o: t_ag(q, o).wait_recv())
+        each(1, n_y, lambda o: t_ya(q, o).wait_recv())
         for j in range(n_sp):
-            dw_ref[q * span : (q + 1) * span, j * width : (j + 1) * width] = ag[q, j]
+            dw_ref[q * span : (q + 1) * span, j * width : (j + 1) * width] = ag[q, j // n_z, j % n_z]
 
     each(1, n_dev, lambda o: t_s2(o).wait_recv())
     sm_ref[...] = srecv[n_dev : 2 * n_dev]
@@ -320,14 +370,18 @@
     w_own().wait_send()
     for k in range(1, pairs):
         w_x(k).wait_send()
-        each(1, n_sp, lambda o: w_sp(k, o).wait_send())
+        w_z(k).wait_send()
+        each(1, n_y, lambda o: w_y(k, 0, o).wait_send())
+        each(1, n_y, lambda o: w_y(k, 1, o).wait_send())
         w_fw(k).wait_send()
         each(0, gpc, lambda q: t_x(k, q).wait_send())
     for k in range(pairs):
         each(0, gpc, lambda q: t_core(k, q).wait_send())
     for q in range(gpc):
-        each(1, n_sp, lambda o: t_rs(q, o).wait_send())
-        each(1, n_sp, lambda o: t_ag(q, o).wait_send())
+        each(1, n_y, lambda o: t_yr(q, o).wait_send())
+        each(1, n_z, lambda o: t_zr(q, o).wait_send())
+        each(1, n_z, lambda o: t_za(q, o).wait_send())
+        each(1, n_y, lambda o: t_ya(q, o).wait_send())
     each(1, n_dev, lambda o: t_s2(o).wait_send())
 
 
@@ -343,16 +397,22 @@
     part_rows = span // per
     shard = w_out.shape[0]
     pairs = n_dp // 2
-    dims = (n_sp, n_dp, gpc, span, chans, width, rows)
+    n_y = 1
+    while 4 * n_y * n_y <= n_sp:
+        n_y *= 2
+    n_z = n_sp // n_y
+    dims = (n_y, n_z, n_dp, gpc, span, chans, width, rows)
     dma = pltpu.SemaphoreType.DMA
     vm = pltpu.VMEM
-    piece = (n_sp, span, width)
+    piece = (n_y, n_z, span, width)
+    w_piece = (n_y, 2, shard // (2 * n_y), depth)
     scratch = [
-        vm((n_dp, n_sp, shard // n_sp, depth), BF16),
+        vm((n_dp,) + w_piece, BF16),
         vm((groups,) + piece, BF16),
         vm((pairs, gpc) + piece, BF16),
         vm((pairs, gpc) + piece, BF16),
         vm((gpc,) + piece, BF16),
+        vm((gpc,) + piece[1:2] + piece[2:], BF16),
         vm((gpc,) + piece, BF16),
         vm((rows, 2 * chans), BF16),
         vm((2 * chans, rows), BF16),
@@ -363,12 +423,15 @@
         vm((2 * n_dev, part_rows + 16, chans), BF16),
         dma, dma,
         dma((pairs,)), dma((pairs,)),
-        dma((pairs, n_sp)), dma((pairs, n_sp)),
+        dma((pairs,)), dma((pairs,)),
+        dma((pairs, 2, n_y)), dma((pairs, 2, n_y)),
         dma((pairs,)), dma((pairs,)),
         dma((pairs, gpc)), dma((pairs, gpc)),
         dma((pairs, gpc)), dma((pairs, gpc)),
-        dma((gpc, n_sp)), dma((gpc, n_sp)),
-        dma((gpc, n_sp)), dma((gpc, n_sp)),
+        dma((gpc, n_y)), dma((gpc, n_y)),
+        dma((gpc, n_z)), dma((gpc, n_z)),
+        dma((gpc, n_z)), dma((gpc, n_z)),
+        dma((gpc, n_y)), dma((gpc, n_y)),
         dma((n_dev,)), dma((n_dev,)),
         dma((n_dev,)), dma((n_dev,)),
     ]
@@ -389,7 +452,7 @@
         u_pre[0], v_pre[0], d_out[0], w_mix,
         jnp.broadcast_to(mix_bias[:, :, None], (groups, span, chans)),
         norm_gain[:, None, :], norm_shift[:, None, :],
-        w_out.reshape(n_sp, shard // n_sp, depth),
+        w_out.reshape(w_piece),
     )
     grad_w = sm[:, :part_rows].reshape(groups, span, span).astype(F32)
     extra = sm.reshape(groups, per, part_rows + 16, chans)[:, 0, part_rows:].astype(F32)

time: 237 us -> 158 us (0.67)
  Pallas kernels: 221 us -> 144 us
    pallas_call x1, Pallas kernels: 221 us -> 144 us  [on_device(): pl.pallas_call(functools.partial(kernel, dims), out_shape=(jax.ShapeDtype...]
where the time goes in v2:
time: 158 us
  Pallas kernels  144 us (91%)
  local copies, waits for them, and re-layouts  8.39 us (5%)
  other arithmetic  5.37 us (3%)
    pallas_call x1, Pallas kernels, on_device(): pl.pallas_call(functools.partial(kernel, dims), out_shape=(jax.ShapeDtype...  144 us
    unnamed x8, local copies, waits for them, and re-layouts  5.72 us
    convert_element_type x1, other arithmetic, on_device(): dw.astype(F32)  4.28 us

profile of v2, /device:TPU:27, one launch (start us, length us, event | category | flops | bytes accessed | tf_op | source)
XLA Modules:
  0.0 158.0 jit_solution(14875311556353059295)
XLA Ops:
  0.6 2.0 %broadcast_in_dim.18.bias_ref = f32[16,128,128]{2,1,0:T(8,128)} broadcast(f32[16,128]{1,0:T(8,128)} %param.12), dimensions={0,1} | broadcast | bytes 1056768 | tf_op jit(solution)/shard_map/broadcast_in_dim | solution.py:453
  2.6 143.6 %shard_map.135 = (bf16[1024,2048]{1,0:T(8,128)(2,1)}, bf16[1024,2048]{1,0:T(8,128)(2,1)}, bf16[512,2048]{1,0:T(8,128)(2,1)}, bf16[32,80,128]{2,1,0:T(8,128)(2,1)}) custom-call(bf16[1024,2048]{1,0:T(8,128)(2,1)} %bitcast.24, bf16[1024,2048]{1,0:T(8,128)(2,1)} %bitcast.25, bf16[1024,2048]{1,0:T(8,128)(2,1)} %bitcast.26, bf16[16,128,128]{2,1,0:T(8,128)(2,1)} %wmix_ref.1, ...), custom_call_target="tpu_custom_call" | custom-call | tf_op jit(solution)/shard_map/pallas_call | solution.py:439
  146.2 0.0 copy-start.2
  146.2 0.0 copy-start.1
  146.2 4.3 %convert_element_type.15 = f32[512,2048]{1,0:T(8,128)} convert(bf16[512,2048]{1,0:T(8,128)(2,1)} %get-tuple-element.13) | non-fusion elementwise | flops 1048576 | bytes 6291456 | tf_op jit(solution)/shard_map/convert_element_type | solution.py:459
  150.5 0.0 copy-done.2
  150.5 0.1 slice.15
  150.6 1.1 bitcast_convert_fusion
  151.7 0.6 slice_bitcast_fusion
  152.3 0.0 copy-done.1
  152.3 0.0 copy-start
  152.3 2.1 %copy.22 = bf16[1,1024,2048]{2,1,0:T(8,128)(2,1)} copy(bf16[1,1024,2048]{2,1,0:T(8,128)(2,1)S(1)} %bitcast.28) | data formatting | bytes 8388608
  154.4 1.6 copy-done
  156.0 2.0 %copy.23 = bf16[1,1024,2048]{2,1,0:T(8,128)(2,1)} copy(bf16[1,1024,2048]{2,1,0:T(8,128)(2,1)S(1)} %bitcast.27) | data formatting | bytes 8388608
  (2 shorter events, 0.0 us)
Async XLA Ops:
  146.2 4.3 %copy-start.2 = (bf16[32,80,128]{2,1,0:T(8,128)(2,1)S(1)}, bf16[32,80,128]{2,1,0:T(8,128)(2,1)}, u32[]{:S(2)}) copy-start(bf16[32,80,128]{2,1,0:T(8,128)(2,1)} %get-tuple-element.14) | copy-start | bytes 1966084
  146.2 6.1 %copy-start.1 = (bf16[1024,2048]{1,0:T(8,128)(2,1)S(1)}, bf16[1024,2048]{1,0:T(8,128)(2,1)}, u32[]{:S(2)}) copy-start(bf16[1024,2048]{1,0:T(8,128)(2,1)} %get-tuple-element.11) | copy-start | bytes 12582916
  152.3 3.7 %copy-start = (bf16[1024,2048]{1,0:T(8,128)(2,1)S(1)}, bf16[1024,2048]{1,0:T(8,128)(2,1)}, u32[]{:S(2)}) copy-start(bf16[1024,2048]{1,0:T(8,128)(2,1)} %get-tuple-element.12) | copy-start | bytes 12582916

commit v3 on v2

--- a/solution.py
+++ b/solution.py
@@ -44,8 +44,9 @@
 
 def kernel(
     dims,
-    u_ref, v_ref, d_ref, wmix_ref, bias_ref, gain_ref, shift_ref, w_ref,
-    gu_ref, gv_ref, dw_ref, sm_ref,
+    u_hbm, v_hbm, d_hbm, wmix_ref, bias_ref, gain_ref, shift_ref, w_ref,
+    gu_hbm, gv_hbm, dw_ref, sm_ref,
+    u_ref, v_ref, d_ref, gu_ref, gv_ref, in_s, gu_s, gv_s,
     wfull, part, rcore, rx, ry, rz, ag, gs, got, wl_ref, wlt_ref, acc, sbuf, srecv,
     wown_s, wown_r, wx_s, wx_r, wz_s, wz_r, wy_s, wy_r, wfw_s, wfw_r,
     core_s, core_r, xs_s, xs_r, yr_s, yr_r, zr_s, zr_r, za_s, za_r, ya_s, ya_r,
@@ -146,6 +147,22 @@
     col = lax.broadcasted_iota(jnp.int32, (span, span), 1)
     lower = row >= col
 
+    loads = [
+        pltpu.make_async_copy(src, dst, in_s.at[n])
+        for n, (src, dst) in enumerate(((v_hbm, v_ref), (u_hbm, u_ref), (d_hbm, d_ref)))
+    ]
+    for load in loads:
+        load.start()
+    barrier = pltpu.get_barrier_semaphore()
+
+    def greet(o):
+        to = (me + o) % n_dev
+        pl.semaphore_signal(
+            barrier, inc=1, device_id={"sp": to // n_dp, "dp": to % n_dp},
+            device_id_type=pl.DeviceIdType.MESH,
+        )
+    each(1, n_dev, greet)
+    pl.semaphore_wait(barrier, n_dev - 1)
     w_own().start()
     for k in range(1, pairs):
         w_x(k).start()
@@ -197,6 +214,8 @@
             core_sum((last // gpc + 1) % pairs, last % gpc)
 
     n_far = (pairs - 1) * gpc
+    for load in loads:
+        load.wait()
     each(0, n_far // 2, forward_step)
     for k in range(1, pairs):
         w_x(k).wait_recv()
@@ -296,9 +315,25 @@
         r16 = lax.broadcasted_iota(jnp.int32, (16, chans), 0)
         extra = jnp.where(r16 == 0, g_bias, jnp.where(r16 == 1, g_gain, jnp.where(r16 == 2, g_shift, 0.0)))
         sbuf[g * per, part_rows : part_rows + 16, :] = extra.astype(BF16)
+        for p in range(per):
+            to = g * per + p
+
+            @pl.when(to != me)
+            def _(to=to):
+                t_s1((to + n_dev - me) % n_dev).start()
 
     per_chunk = gpc // 2
     flat = wfull.reshape(n_dp, wfull.shape[1] * 2 * wfull.shape[3], wfull.shape[4])
+
+    def stores(i):
+        turn = i // per_chunk
+        chunk = 2 * down(turn // 2) + (c + turn) % 2
+        first = (chunk * gpc + 2 * (i % per_chunk)) * chans
+        at = pl.ds(pl.multiple_of(first, 2 * chans), 2 * chans)
+        return (
+            pltpu.make_async_copy(gu_ref.at[:, at], gu_hbm.at[:, at], gu_s.at[i]),
+            pltpu.make_async_copy(gv_ref.at[:, at], gv_hbm.at[:, at], gv_s.at[i]),
+        )
 
     def backward_step(i):
         turn = i // per_chunk
@@ -312,6 +347,8 @@
             gs[at, :] = mm(d_ref[at, :], wrows, 1, 1).astype(BF16)
         each(0, rows // (2 * span), one)
         each(0, 2, lambda h: backward_group(chunk * gpc + 2 * two + h, h))
+        for store in stores(i):
+            store.start()
 
     n_steps = n_dp * per_chunk
     actions = {}
@@ -348,8 +385,7 @@
 
     each(0, n_steps, whole_step)
 
-    each(1, n_dev, lambda o: t_s1(o).start())
-    for fn in late:
+    for fn in late[:2]:
         fn()
     each(1, n_dev, lambda o: t_s1(o).wait_recv())
     acc_s = sbuf[me].astype(F32)
@@ -358,6 +394,8 @@
     sbuf[me] = acc_s.astype(BF16)
     srecv[n_dev + me] = acc_s.astype(BF16)
     each(1, n_dev, lambda o: t_s2(o).start())
+    for fn in late[2:]:
+        fn()
 
     for q in range(gpc):
         each(1, n_y, lambda o: t_ya(q, o).wait_recv())
@@ -366,6 +404,11 @@
 
     each(1, n_dev, lambda o: t_s2(o).wait_recv())
     sm_ref[...] = srecv[n_dev : 2 * n_dev]
+
+    def stored(i):
+        for store in stores(i):
+            store.wait()
+    each(0, n_steps, stored)
 
     w_own().wait_send()
     for k in range(1, pairs):
@@ -406,7 +449,11 @@
     vm = pltpu.VMEM
     piece = (n_y, n_z, span, width)
     w_piece = (n_y, 2, shard // (2 * n_y), depth)
+    n_steps = groups // 2
     scratch = [
+        vm((rows, wide), BF16), vm((rows, wide), BF16), vm((rows, depth), BF16),
+        vm((rows, wide), BF16), vm((rows, wide), BF16),
+        dma((3,)), dma((n_steps,)), dma((n_steps,)),
         vm((n_dp,) + w_piece, BF16),
         vm((groups,) + piece, BF16),
         vm((pairs, gpc) + piece, BF16),
@@ -436,6 +483,7 @@
         dma((n_dev,)), dma((n_dev,)),
     ]
     spec = pl.BlockSpec(memory_space=pltpu.VMEM)
+    hbm = pl.BlockSpec(memory_space=pl.ANY)
     gu, gv, dw, sm = pl.pallas_call(
         functools.partial(kernel, dims),
         out_shape=(
@@ -444,10 +492,10 @@
             jax.ShapeDtypeStruct((shard, depth), BF16),
             jax.ShapeDtypeStruct((n_dev, part_rows + 16, chans), BF16),
         ),
-        in_specs=[spec] * 8,
-        out_specs=(spec,) * 4,
+        in_specs=[hbm] * 3 + [spec] * 5,
+        out_specs=(hbm, hbm, spec, spec),
         scratch_shapes=scratch,
-        compiler_params=pltpu.CompilerParams(has_side_effects=True, vmem_limit_bytes=67043328),
+        compiler_params=pltpu.CompilerParams(collective_id=0, has_side_effects=True, vmem_limit_bytes=67043328),
     )(
         u_pre[0], v_pre[0], d_out[0], w_mix,
         jnp.broadcast_to(mix_bias[:, :, None], (groups, span, chans)),

time: 158 us -> 158 us (level)
  Pallas kernels: 144 us -> 142 us
where the time goes in v3:
time: 158 us; the launch traced here: 157 us
  Pallas kernels  142 us (90%)
  local copies, waits for them, and re-layouts  8.39 us (5%)
  other arithmetic  5.37 us (3%)
    pallas_call x1, Pallas kernels, on_device(): pl.pallas_call(functools.partial(kernel, dims), out_shape=(jax.ShapeDtype...  142 us
    unnamed x8, local copies, waits for them, and re-layouts  5.72 us
    convert_element_type x1, other arithmetic, on_device(): dw.astype(F32)  4.28 us

profile of v3, /device:TPU:27, one launch (start us, length us, event | category | flops | bytes accessed | tf_op | source)
XLA Modules:
  0.0 156.9 jit_solution(1168826026070746773)
XLA Ops:
  0.6 2.0 %broadcast_in_dim.18.bias_ref = f32[16,128,128]{2,1,0:T(8,128)} broadcast(f32[16,128]{1,0:T(8,128)} %param.12), dimensions={0,1} | broadcast | bytes 1056768 | tf_op jit(solution)/shard_map/broadcast_in_dim | solution.py:501
  2.6 142.5 %shard_map.135 = (bf16[1024,2048]{1,0:T(8,128)(2,1)}, bf16[1024,2048]{1,0:T(8,128)(2,1)}, bf16[512,2048]{1,0:T(8,128)(2,1)}, bf16[32,80,128]{2,1,0:T(8,128)(2,1)}) custom-call(bf16[1024,2048]{1,0:T(8,128)(2,1)} %bitcast.24, bf16[1024,2048]{1,0:T(8,128)(2,1)} %bitcast.25, bf16[1024,2048]{1,0:T(8,128)(2,1)} %bitcast.26, bf16[16,128,128]{2,1,0:T(8,128)(2,1)} %wmix_ref.1, ...), custom_call_target="tpu_custom_call" | custom-call | tf_op jit(solution)/shard_map/pallas_call | solution.py:487
  145.1 0.0 copy-start.2
  145.1 0.0 copy-start.1
  145.1 4.3 %convert_element_type.15 = f32[512,2048]{1,0:T(8,128)} convert(bf16[512,2048]{1,0:T(8,128)(2,1)} %get-tuple-element.13) | non-fusion elementwise | flops 1048576 | bytes 6291456 | tf_op jit(solution)/shard_map/convert_element_type | solution.py:507
  149.4 0.0 copy-done.2
  149.4 0.1 slice.15
  149.5 1.1 bitcast_convert_fusion
  150.6 0.6 slice_bitcast_fusion
  151.2 0.0 copy-done.1
  151.2 0.0 copy-start
  151.2 2.1 %copy.22 = bf16[1,1024,2048]{2,1,0:T(8,128)(2,1)} copy(bf16[1,1024,2048]{2,1,0:T(8,128)(2,1)S(1)} %bitcast.28) | data formatting | bytes 8388608
  153.3 1.6 copy-done
  154.9 2.0 %copy.23 = bf16[1,1024,2048]{2,1,0:T(8,128)(2,1)} copy(bf16[1,1024,2048]{2,1,0:T(8,128)(2,1)S(1)} %bitcast.27) | data formatting | bytes 8388608
  (2 shorter events, 0.0 us)
Async XLA Ops:
  145.1 4.3 %copy-start.2 = (bf16[32,80,128]{2,1,0:T(8,128)(2,1)S(1)}, bf16[32,80,128]{2,1,0:T(8,128)(2,1)}, u32[]{:S(2)}) copy-start(bf16[32,80,128]{2,1,0:T(8,128)(2,1)} %get-tuple-element.14) | copy-start | bytes 1966084
  145.1 6.1 %copy-start.1 = (bf16[1024,2048]{1,0:T(8,128)(2,1)S(1)}, bf16[1024,2048]{1,0:T(8,128)(2,1)}, u32[]{:S(2)}) copy-start(bf16[1024,2048]{1,0:T(8,128)(2,1)} %get-tuple-element.11) | copy-start | bytes 12582916
  151.2 3.7 %copy-start = (bf16[1024,2048]{1,0:T(8,128)(2,1)S(1)}, bf16[1024,2048]{1,0:T(8,128)(2,1)}, u32[]{:S(2)}) copy-start(bf16[1024,2048]{1,0:T(8,128)(2,1)} %get-tuple-element.12) | copy-start | bytes 12582916
